TPU v7x, 512 devices: a 4x2x32 block of a 4x8x32 slice. The times are simulated.
512 devices in a mesh: grp: 2 (over y), sp: 64 (over z, core), tp: 4 (over x).
Axes of the slice: x: 4, y: 2, z: 32, core: 2. Of those that a mesh axis runs over, the one named last changes fastest.
The devices are a block of a 4x8x32 slice.
Arguments:
- tokens: bfloat16 [65536, 2048], P(('grp', 'sp')), parts along dimension 0, may hold values from -6 to 6
- gate_in: bfloat16 [2, 2048, 512], P(None, 'sp', 'tp'), may hold values from -0.125 to 0.125
- gate_conv: bfloat16 [2, 2048, 512], P(None, 'sp', 'tp'), may hold values from -0.125 to 0.125
- value_in: bfloat16 [2, 2048, 512], P(None, 'sp', 'tp'), may hold values from -0.125 to 0.125
- out_weight: bfloat16 [2, 512, 2048], P(None, None, 'sp'), may hold values from -0.25 to 0.25
- conv_taps: float32 [2, 3, 512], replicated, may hold values from -7 to 7
- pre_gain: float32 [2, 2048], replicated, may hold values from 0.1 to 1.9
- mix_gain: float32 [2, 512], replicated, may hold values from 0.1 to 1.9
- post_gain: float32 [2, 2048], replicated, may hold values from 0.1 to 1.9
Outputs:
- result: bfloat16 [65536, 2048], P(('grp', 'sp', 'tp')), parts along dimension 0
There are 2 independent parts, one for each index of `grp`. A program takes and returns all parts, laid end to end along the dimension named above; an argument that names none is the same for every part. Nothing has to cross between parts.
All inputs are finite; a program needn't handle non-finite values.
Results may differ from a plain program's by a relative error of at most 0.011.
Values may be sent and summed in bfloat16 or wider, within the bound.
No kernel may reach another device: no remote copies, remote signals or barrier semaphores. Data moves between devices by JAX's collectives and lax.ppermute only.
A program may use at most 64 MiB of HBM per device.

v0:
```python
import jax
import jax.numpy as jnp
from jax import lax
from jax.sharding import PartitionSpec as P

EPS = 1e-06
GATE_SCALE = 2.0**18
OUT_SCALE = 2.0**17


def passed_along(x, axis, by):
    length = lax.axis_size(axis)
    pairs = [(i, i + by) for i in range(length) if 0 <= i + by < length]
    return lax.ppermute(x, axis, pairs)


def rms_norm(values, gain):
    return values * lax.rsqrt(jnp.mean(values * values, axis=-1, keepdims=True) + EPS) * gain


def stored(values):
    return lax.optimization_barrier(values.astype(jnp.bfloat16))


def sent(values, scale):
    return (values.astype(jnp.float32) * scale).astype(jnp.float16)


def received(values, scale):
    return stored(values.astype(jnp.float32) * (1.0 / scale))


def per_device(
    tokens, gate_in, gate_conv, value_in, out_weight, conv_taps, pre_gain, mix_gain, post_gain
):
    layer_count = gate_in.shape[0]
    channel_count = gate_in.shape[2]
    whole_count = out_weight.shape[1]
    tap_count = conv_taps.shape[1]
    row_count = tokens.shape[0]
    tp_size = lax.axis_size("tp")
    tp_index = lax.axis_index("tp")
    row_share = row_count // tp_size
    pieces = []
    for layer_index in range(layer_count):
        for w in (gate_in, gate_conv, value_in):
            pieces.append(sent(w[layer_index], GATE_SCALE))
        pieces.append(sent(out_weight[layer_index].T, OUT_SCALE))
    packed = jnp.concatenate(pieces, axis=1)
    whole = lax.all_gather(packed, "sp", axis=0, tiled=True)
    stream = tokens.astype(jnp.float32)
    start = 0
    for layer_index in range(layer_count):
        is_last = layer_index == layer_count - 1
        gates = received(whole[:, start : start + 3 * channel_count], GATE_SCALE)
        start += 3 * channel_count
        out_whole = received(whole[:, start : start + whole_count], OUT_SCALE)
        start += whole_count
        normed = stored(rms_norm(stream, pre_gain[layer_index]))
        mixers = stored(jnp.dot(normed, gates, preferred_element_type=jnp.float32))
        outer = mixers[:, :channel_count]
        inner = mixers[:, channel_count : 2 * channel_count]
        values = mixers[:, 2 * channel_count :]
        gated = stored(inner.astype(jnp.float32) * values.astype(jnp.float32))
        before = passed_along(gated[row_count - (tap_count - 1) :], "sp", 1)
        padded = jnp.concatenate([before, gated], axis=0)
        taps_here = lax.dynamic_slice_in_dim(
            conv_taps[layer_index], tp_index * channel_count, channel_count, 1
        )
        filtered = jnp.zeros((row_count, channel_count), jnp.float32)
        for tap_index in range(tap_count):
            filtered = filtered + taps_here[tap_index] * padded[
                tap_index : tap_index + row_count
            ].astype(jnp.float32)
        mixed_raw = stored(outer.astype(jnp.float32) * filtered)
        if is_last:
            arrived = lax.all_to_all(mixed_raw, "tp", split_axis=0, concat_axis=1, tiled=True)
            residual = lax.dynamic_slice_in_dim(stream, tp_index * row_share, row_share, 0)
        else:
            arrived = lax.all_gather(mixed_raw, "tp", axis=1, tiled=True)
            residual = stream
        mixed = stored(rms_norm(arrived.astype(jnp.float32), mix_gain[layer_index]))
        branch = stored(
            lax.dot_general(
                mixed, out_whole, (((1,), (1,)), ((), ())), preferred_element_type=jnp.float32
            )
        )
        stream = residual + rms_norm(branch.astype(jnp.float32), post_gain[layer_index])
    return stream.astype(jnp.bfloat16)


def solution(mesh):
    placed = (
        P(("grp", "sp"), None),
        P(None, "sp", "tp"),
        P(None, "sp", "tp"),
        P(None, "sp", "tp"),
        P(None, None, "sp"),
        P(),
        P(),
        P(),
        P(),
    )
    return jax.shard_map(
        per_device,
        mesh=mesh,
        in_specs=placed,
        out_specs=P(("grp", "sp", "tp"), None),
        check_vma=False,
    )
```

profile of v0, /device:TPU:33, one launch (start us, length us, event | category | flops | bytes accessed | tf_op | source)
XLA Modules:
  0.0 175.5 jit_solution(6006410904357195028)
XLA Ops:
  0.0 0.7 constant_dynamic-update-slice_fusion.5
  0.7 0.7 constant_dynamic-update-slice_fusion.4
  1.4 0.7 constant_dynamic-update-slice_fusion.3
  2.1 0.8 fusion.17
  2.9 0.7 constant_dynamic-update-slice_fusion.2
  3.6 0.7 constant_dynamic-update-slice_fusion.1
  4.3 0.7 constant_dynamic-update-slice_fusion
  5.0 0.8 fusion.19
  5.8 121.4 %all-gather.1 = f16[2048,1792]{1,0:T(8,128)(2,1)S(1)} all-gather(f16[32,1792]{1,0:T(8,128)(2,1)S(1)} %fusion.19), channel_id=1, replica_groups=mesh['grp'=2,'sp'=64,'tp'=4] {'sp'}, dimensions={0}, use_global_device_ids=true | all-gather | bytes 7454720 | tf_op jit(solution)/shard_map/all_gather | solution.py:50
  127.2 1.9 %multiply_convert_fusion.3 = (bf16[2048,384]{1,0:T(8,128)(2,1)}, bf16[2048,384]{1,0:T(8,128)(2,1)S(1)}) fusion(f16[2048,1792]{1,0:T(8,128)(2,1)S(1)} %all-gather.1), kind=kLoop, calls=%fused_computation.14 | loop fusion | flops 4718592 | bytes 6291456 | tf_op jit(solution)/shard_map/convert_element_type | solution.py:22
  129.1 0.0 copy-done.5
  129.1 0.0 copy-done.1
  129.1 0.5 fusion.2
  129.6 0.6 fusion.4
  130.1 1.2 convolution_convert_fusion.3
  131.5 2.3 %collective-permute-start = (bf16[2,128]{1,0:T(2,128)(2,1)S(1)}, bf16[2,128]{1,0:T(2,128)(2,1)S(1)}, u32[]{:S(2)}, u32[]{:S(2)}) collective-permute-start(bf16[2,128]{1,0:T(2,128)(2,1)S(1)} %slice.162), channel_id=1, source_target_pairs={{0,4},{4,8},{8,12},{12,16},{16,20},{20,24},{24,28},{28,32},{32,36}... | collective-permute-start | bytes 1544 | tf_op jit(solution)/shard_map/ppermute | solution.py:14
  133.7 0.0 copy-start.7
  133.7 0.0 copy-start.8
  133.8 0.0 copy-start.6
  133.8 3.0 %multiply_convert_fusion = (bf16[2048,512]{1,0:T(8,128)(2,1)}, bf16[2048,512]{1,0:T(8,128)(2,1)}) fusion(f16[2048,1792]{1,0:T(8,128)(2,1)S(1)} %all-gather.1), kind=kLoop, calls=%fused_computation.10 | loop fusion | flops 6291456 | bytes 8388608 | tf_op jit(solution)/shard_map/convert_element_type | solution.py:22
  136.8 0.0 copy-done.7
  136.8 0.0 copy-done.8
  136.8 0.0 copy-done.6
  136.8 0.0 copy-start.3
  136.9 0.0 collective-permute-done
  136.9 0.1 multiply_convert_fusion.7
  137.0 13.2 %all_gather.7 = bf16[512,512]{1,0:T(8,128)(2,1)S(1)} all-gather(bf16[512,128]{1,0:T(8,128)(2,1)S(1)} %multiply_convert_fusion.7), channel_id=1, replica_groups=mesh['grp'=2,'sp'=64,'tp'=4] {'tp'}, dimensions={1}, use_global_device_ids=true | all-gather | bytes 655360 | tf_op jit(solution)/shard_map/all_gather | solution.py:80
  150.2 0.2 fusion.5
  150.4 0.2 fusion.7
  150.6 1.3 convolution_convert_fusion
  151.9 0.5 fusion
  152.4 1.1 multiply_reduce_fusion
  153.5 0.0 copy-start.4
  153.5 0.4 multiply_convert_fusion.1
  154.0 1.5 copy-done
  155.5 0.6 copy-done.4
  156.1 1.2 convolution_convert_fusion.2
  157.4 4.3 %collective-permute-start.1 = (bf16[2,128]{1,0:T(2,128)(2,1)S(1)}, bf16[2,128]{1,0:T(2,128)(2,1)S(1)}, u32[]{:S(2)}, u32[]{:S(2)}) collective-permute-start(bf16[2,128]{1,0:T(2,128)(2,1)S(1)} %slice.170), channel_id=1, source_target_pairs={{0,4},{4,8},{8,12},{12,16},{16,20},{20,24},{24,28},{28,32},{32,36}... | collective-permute-start | bytes 1544 | tf_op jit(solution)/shard_map/ppermute | solution.py:14
  161.7 0.7 collective-permute-done.1
  162.4 0.1 multiply_convert_fusion.5
  162.5 0.8 copy.10
  163.3 3.4 %all-to-all-start = ((bf16[4,128,128]{1,2,0:T(8,128)(2,1)}), bf16[4,128,128]{1,2,0:T(8,128)(2,1)S(1)}, u32[]{:S(2)}, u32[]{:S(2)}) async-start(bf16[4,128,128]{1,2,0:T(8,128)(2,1)} %copy.10), calls=%async_computation | async-start | bytes 262144 | tf_op jit(solution)/shard_map/all_to_all | solution.py:77
  166.7 5.2 %all-to-all-done = bf16[4,128,128]{1,2,0:T(8,128)(2,1)S(1)} async-done(((bf16[4,128,128]{1,2,0:T(8,128)(2,1)}), bf16[4,128,128]{1,2,0:T(8,128)(2,1)S(1)}, u32[]{:S(2)}, u32[]{:S(2)}) %all-to-all-start) | async-done | bytes 131104 | tf_op jit(solution)/shard_map/all_to_all | solution.py:77
  172.0 0.1 multiply_reduce_fusion.1
  172.1 0.1 fusion.13
  172.2 0.8 convolution_convert_fusion.1
  173.0 0.2 fusion.8
  173.2 2.2 %fusion.11 = bf16[128,2048]{1,0:T(8,128)(2,1)} fusion(bf16[128,2048]{1,0:T(8,128)(2,1)S(1)} %convolution_convert_fusion.1, f32[512,2048]{1,0:T(8,128)} %copy-done, s32[]{:T(128)S(6)} %select_n.2, f32[2048]{0:T(1024)S(1)} %bitcast.72, f32[128]{0:T(128)S(1)} %add_rsqrt_fusion.4), kind=kLoop, calls=%fused_computation.30 | loop fusion | flops 1310720 | bytes 2105860 | tf_op jit(solution)/shard_map/convert_element_type | solution.py:89
  (22 shorter events, 0.2 us)
Async XLA Ops:
  127.2 1.9 %copy-start.5 = (f32[2,2048]{1,0:T(2,128)S(1)}, f32[2,2048]{1,0:T(2,128)}, u32[]{:S(2)}) copy-start(f32[2,2048]{1,0:T(2,128)} %param.15) | copy-start | bytes 49156
  127.2 1.9 %copy-start.1 = (bf16[512,2048]{1,0:T(8,128)(2,1)S(1)}, bf16[512,2048]{1,0:T(8,128)(2,1)}, u32[]{:S(2)}) copy-start(bf16[512,2048]{1,0:T(8,128)(2,1)} %param.9) | copy-start | bytes 6291460
  131.5 5.4 %collective-permute-start = (bf16[2,128]{1,0:T(2,128)(2,1)S(1)}, bf16[2,128]{1,0:T(2,128)(2,1)S(1)}, u32[]{:S(2)}, u32[]{:S(2)}) collective-permute-start(bf16[2,128]{1,0:T(2,128)(2,1)S(1)} %slice.162), channel_id=1, source_target_pairs={{0,4},{4,8},{8,12},{12,16},{16,20},{20,24},{24,28},{28,32},{32,36}... | collective-permute-start | bytes 1544 | tf_op jit(solution)/shard_map/ppermute | solution.py:14
  133.7 3.0 %copy-start.7 = (f32[2,3,512]{2,0,1:T(2,128)S(1)}, f32[2,3,512]{2,0,1:T(2,128)}, u32[]{:S(2)}) copy-start(f32[2,3,512]{2,0,1:T(2,128)} %param.14) | copy-start | bytes 36868
  133.7 3.0 %copy-start.8 = (f32[2,512]{1,0:T(2,128)S(1)}, f32[2,512]{1,0:T(2,128)}, u32[]{:S(2)}) copy-start(f32[2,512]{1,0:T(2,128)} %param.16) | copy-start | bytes 12292
  133.8 3.0 %copy-start.6 = (f32[2,2048]{1,0:T(2,128)S(1)}, f32[2,2048]{1,0:T(2,128)}, u32[]{:S(2)}) copy-start(f32[2,2048]{1,0:T(2,128)} %param.17) | copy-start | bytes 49156
  136.8 13.8 %copy-start.3 = (bf16[2048,512]{1,0:T(8,128)(2,1)S(1)}, bf16[2048,512]{1,0:T(8,128)(2,1)}, u32[]{:S(2)}) copy-start(bf16[2048,512]{1,0:T(8,128)(2,1)} %get-tuple-element.8) | copy-start | bytes 6291460
  153.5 2.0 %copy-start = (f32[512,2048]{1,0:T(8,128)}, f32[512,2048]{1,0:T(8,128)S(1)}, u32[]{:S(2)}) copy-start(f32[512,2048]{1,0:T(8,128)S(1)} %get-tuple-element.6) | copy-start | bytes 12582916
  153.5 2.6 %copy-start.4 = (bf16[2048,384]{1,0:T(8,128)(2,1)S(1)}, bf16[2048,384]{1,0:T(8,128)(2,1)}, u32[]{:S(2)}) copy-start(bf16[2048,384]{1,0:T(8,128)(2,1)} %get-tuple-element.9) | copy-start | bytes 4718596
  156.1 16.1 %copy-start.2 = (bf16[2048,512]{1,0:T(8,128)(2,1)S(1)}, bf16[2048,512]{1,0:T(8,128)(2,1)}, u32[]{:S(2)}) copy-start(bf16[2048,512]{1,0:T(8,128)(2,1)} %get-tuple-element.7) | copy-start | bytes 6291460
  157.4 5.0 %collective-permute-start.1 = (bf16[2,128]{1,0:T(2,128)(2,1)S(1)}, bf16[2,128]{1,0:T(2,128)(2,1)S(1)}, u32[]{:S(2)}, u32[]{:S(2)}) collective-permute-start(bf16[2,128]{1,0:T(2,128)(2,1)S(1)} %slice.170), channel_id=1, source_target_pairs={{0,4},{4,8},{8,12},{12,16},{16,20},{20,24},{24,28},{28,32},{32,36}... | collective-permute-start | bytes 1544 | tf_op jit(solution)/shard_map/ppermute | solution.py:14
  163.3 8.7 %all-to-all-start = ((bf16[4,128,128]{1,2,0:T(8,128)(2,1)}), bf16[4,128,128]{1,2,0:T(8,128)(2,1)S(1)}, u32[]{:S(2)}, u32[]{:S(2)}) async-start(bf16[4,128,128]{1,2,0:T(8,128)(2,1)} %copy.10), calls=%async_computation | async-start | bytes 262144 | tf_op jit(solution)/shard_map/all_to_all | solution.py:77
where the time goes:
time: 176 us; the launch traced here: 175 us
  blocking collectives  135 us (77%)
  other arithmetic  17.1 us (10%)
  starting transfers between devices  9.95 us (6%)
  waiting for transfers between devices  5.92 us (3%)
  matrix products  4.61 us (3%)
  local copies, waits for them, and re-layouts  3.04 us (2%)
    all_gather x1, blocking collectives, per_device(): whole = lax.all_gather(packed, 'sp', axis=0, tiled=True)  121 us
    all_gather x1, blocking collectives, per_device(): arrived = lax.all_gather(mixed_raw, 'tp', axis=1, tiled=True)  13.2 us
    ppermute x2, starting transfers between devices, passed_along(): return lax.ppermute(x, axis, pairs)  6.53 us
    convert_element_type x10, other arithmetic, stored(): return lax.optimization_barrier(values.astype(jnp.bfloat16))  6.5 us
    all_to_all x1, waiting for transfers between devices, per_device(): lax.all_to_all(mixed_raw, 'tp', split_axis=0, concat_axis=1, tiled=True)  5.24 us
    unnamed x7, other arithmetic  5.02 us
  transfers between devices with their start and end apart: 3, of which 2 were waited for; matrix products, arithmetic and copies ran while one was open for 2% of the time, Pallas kernels for 0%

commit v1 on v0

--- a/solution.py
+++ b/solution.py
@@ -47,7 +47,9 @@
             pieces.append(sent(w[layer_index], GATE_SCALE))
         pieces.append(sent(out_weight[layer_index].T, OUT_SCALE))
     packed = jnp.concatenate(pieces, axis=1)
-    whole = lax.all_gather(packed, "sp", axis=0, tiled=True)
+    whole = jnp.concatenate(
+        lax.all_to_all(jnp.stack([packed] * lax.axis_size("sp")), "sp", 0, 0), axis=0
+    )
     stream = tokens.astype(jnp.float32)
     start = 0
     for layer_index in range(layer_count):

time: 176 us -> 754 us (4.28)
  waiting for transfers between devices: 5.92 us -> 651 us
  blocking collectives: 135 us -> 11.8 us
  starting transfers between devices: 9.95 us -> 57.4 us
    all_to_all x0 -> x1, waiting for transfers between devices: none -> 635 us  [per_device(): lax.all_to_all(jnp.stack([packed] * lax.axis_size('sp')), 'sp', 0, 0)]
    all_gather x1 -> x0, blocking collectives: 121 us -> none  [per_device(): whole = lax.all_gather(packed, 'sp', axis=0, tiled=True)]
    all_to_all x0 -> x1, starting transfers between devices: none -> 47.6 us  [per_device(): lax.all_to_all(jnp.stack([packed] * lax.axis_size('sp')), 'sp', 0, 0)]
    ppermute x2, waiting for transfers between devices: 0.68 us -> 11.8 us  [passed_along(): return lax.ppermute(x, axis, pairs)]
  transfers between devices with their start and end apart: 3 -> 4, of which waited for: 2 -> 4; matrix products, arithmetic and copies ran while one was open for 2% -> 1% of each run, Pallas kernels for 0% -> 0%
where the time goes in v1:
time: 754 us; the launch traced here: 753 us
  waiting for transfers between devices  651 us (86%)
  starting transfers between devices  57.4 us (8%)
  other arithmetic  20.7 us (3%)
  blocking collectives  11.8 us (2%)
    all_to_all x1, waiting for transfers between devices, per_device(): lax.all_to_all(jnp.stack([packed] * lax.axis_size('sp')), 'sp', 0, 0)  635 us
    all_to_all x1, starting transfers between devices, per_device(): lax.all_to_all(jnp.stack([packed] * lax.axis_size('sp')), 'sp', 0, 0)  47.6 us
  transfers between devices with their start and end apart: 4, of which 4 were waited for; matrix products, arithmetic and copies ran while one was open for 1% of the time, Pallas kernels for 0%

profile of v1, /device:TPU:33, one launch (start us, length us, event | category | flops | bytes accessed | tf_op | source)
XLA Modules:
  0.0 752.7 jit_solution(9170751710830120930)
XLA Ops:
  0.0 0.7 constant_dynamic-update-slice_fusion.5
  0.7 0.7 constant_dynamic-update-slice_fusion.4
  1.4 0.7 constant_dynamic-update-slice_fusion.3
  2.1 0.8 fusion.17
  2.9 0.7 constant_dynamic-update-slice_fusion.2
  3.6 0.7 constant_dynamic-update-slice_fusion.1
  4.3 0.7 constant_dynamic-update-slice_fusion
  5.0 0.8 fusion.19
  5.8 3.9 stack.2
  9.7 47.6 %all-to-all-start = ((f16[64,32,1792]{2,1,0:T(8,128)(2,1)}), f16[64,32,1792]{2,1,0:T(8,128)(2,1)}, u32[]{:S(2)}, u32[]{:S(2)}) async-start(f16[64,32,1792]{2,1,0:T(8,128)(2,1)} %stack.2), calls=%async_computation | async-start | bytes 14680064 | tf_op jit(solution)/shard_map/all_to_all | solution.py:51
  57.3 0.0 copy-start.4
  57.3 0.0 copy-done.1
  57.3 0.5 fusion.2
  57.8 0.2 copy-done.4
  58.0 0.0 copy-start.6
  58.1 0.0 copy-start.7
  58.1 0.0 copy-start.5
  58.1 1.9 fusion.4
  59.9 0.0 copy-done.6
  60.0 0.0 copy-done.7
  60.0 0.0 copy-done.5
  60.0 634.7 %all-to-all-done = f16[64,32,1792]{2,1,0:T(8,128)(2,1)} async-done(((f16[64,32,1792]{2,1,0:T(8,128)(2,1)}), f16[64,32,1792]{2,1,0:T(8,128)(2,1)}, u32[]{:S(2)}, u32[]{:S(2)}) %all-to-all-start) | async-done | bytes 7340064 | tf_op jit(solution)/shard_map/all_to_all | solution.py:51
  694.8 2.7 multiply_convert_fusion.3
  697.5 1.2 convolution_convert_fusion.3
  698.8 4.5 collective-permute-start
  703.3 4.5 multiply_convert_fusion
  707.8 5.5 collective-permute-done
  713.3 0.1 multiply_convert_fusion.7
  713.4 11.8 %all_gather.3 = bf16[512,512]{1,0:T(8,128)(2,1)S(1)} all-gather(bf16[512,128]{1,0:T(8,128)(2,1)S(1)} %multiply_convert_fusion.7), channel_id=1, replica_groups=mesh['grp'=2,'sp'=64,'tp'=4] {'tp'}, dimensions={1}, use_global_device_ids=true | all-gather | bytes 655360 | tf_op jit(solution)/shard_map/all_gather | solution.py:82
  725.2 0.2 fusion.5
  725.4 0.2 fusion.7
  725.6 1.3 convolution_convert_fusion
  726.9 0.5 fusion
  727.4 1.1 multiply_reduce_fusion
  728.5 0.4 multiply_convert_fusion.1
  728.9 1.5 copy-done
  730.5 1.2 convolution_convert_fusion.2
  731.8 2.0 collective-permute-start.1
  733.7 6.4 collective-permute-done.1
  740.1 0.1 multiply_convert_fusion.5
  740.2 0.8 copy.10
  741.0 3.4 all-to-all-start.1
  744.4 4.8 all-to-all-done.1
  749.2 0.1 multiply_reduce_fusion.1
  749.3 0.1 fusion.13
  749.4 0.8 convolution_convert_fusion.1
  750.3 0.2 fusion.8
  750.5 2.2 fusion.11
  (22 shorter events, 0.2 us)
Async XLA Ops:
  9.7 47.6 %copy-start.1 = (bf16[512,2048]{1,0:T(8,128)(2,1)S(1)}, bf16[512,2048]{1,0:T(8,128)(2,1)}, u32[]{:S(2)}) copy-start(bf16[512,2048]{1,0:T(8,128)(2,1)} %param.9) | copy-start | bytes 6291460
  9.7 685.1 %all-to-all-start = ((f16[64,32,1792]{2,1,0:T(8,128)(2,1)}), f16[64,32,1792]{2,1,0:T(8,128)(2,1)}, u32[]{:S(2)}, u32[]{:S(2)}) async-start(f16[64,32,1792]{2,1,0:T(8,128)(2,1)} %stack.2), calls=%async_computation | async-start | bytes 14680064 | tf_op jit(solution)/shard_map/all_to_all | solution.py:51
  57.3 0.7 copy-start.4
  58.0 1.9 copy-start.6
  58.1 1.9 copy-start.7
  58.1 1.9 copy-start.5
  694.8 2.7 copy-start.3
  698.8 14.4 %collective-permute-start = (bf16[2,128]{1,0:T(2,128)(2,1)S(1)}, bf16[2,128]{1,0:T(2,128)(2,1)S(1)}, u32[]{:S(2)}, u32[]{:S(2)}) collective-permute-start(bf16[2,128]{1,0:T(2,128)(2,1)S(1)} %slice.162), channel_id=1, source_target_pairs={{0,4},{4,8},{8,12},{12,16},{16,20},{20,24},{24,28},{28,32},{32,36}... | collective-permute-start | bytes 1544 | tf_op jit(solution)/shard_map/ppermute | solution.py:14
  728.5 1.9 copy-start
  730.5 19.0 %copy-start.2 = (bf16[2048,512]{1,0:T(8,128)(2,1)S(1)}, bf16[2048,512]{1,0:T(8,128)(2,1)}, u32[]{:S(2)}) copy-start(bf16[2048,512]{1,0:T(8,128)(2,1)} %get-tuple-element.7) | copy-start | bytes 6291460
  731.8 8.3 %collective-permute-start.1 = (bf16[2,128]{1,0:T(2,128)(2,1)S(1)}, bf16[2,128]{1,0:T(2,128)(2,1)S(1)}, u32[]{:S(2)}, u32[]{:S(2)}) collective-permute-start(bf16[2,128]{1,0:T(2,128)(2,1)S(1)} %slice.170), channel_id=1, source_target_pairs={{0,4},{4,8},{8,12},{12,16},{16,20},{20,24},{24,28},{28,32},{32,36}... | collective-permute-start | bytes 1544 | tf_op jit(solution)/shard_map/ppermute | solution.py:14
  741.0 8.2 %all-to-all-start.1 = ((bf16[4,128,128]{1,2,0:T(8,128)(2,1)}), bf16[4,128,128]{1,2,0:T(8,128)(2,1)S(1)}, u32[]{:S(2)}, u32[]{:S(2)}) async-start(bf16[4,128,128]{1,2,0:T(8,128)(2,1)} %copy.10), calls=%async_computation.1 | async-start | bytes 262144 | tf_op jit(solution)/shard_map/all_to_all | solution.py:79
